TPU v7x, 32 devices: a whole 2x2x4 slice. The times are simulated.
32 devices in a mesh: sp: 4 (over z), fs: 4 (over y, x), tp: 2 (over core).
Axes of the slice: x: 2, y: 2, z: 4, core: 2. Of those that a mesh axis runs over, the one named last changes fastest.
Arguments:
- tokens: bfloat16 [4096, 2048], P(('fs', 'sp')), parts along dimension 0, may hold values from -6 to 6
- norm_gain: float32 [2048], replicated, may hold values from 0.1 to 1.9
- w_query: bfloat16 [2048, 1024], P('sp', 'tp'), may hold values from -0.080939698 to 0.080939698
- w_key: bfloat16 [2048, 256], P('sp', 'tp'), may hold values from -0.080939698 to 0.080939698
- w_value: bfloat16 [2048, 256], P('sp', 'tp'), may hold values from -0.125 to 0.125
- w_conv_in: bfloat16 [2048, 1024], P('sp', 'tp'), may hold values from -0.125 to 0.125
- w_conv_gate: bfloat16 [2048, 1024], P('sp', 'tp'), may hold values from -0.125 to 0.125
- sink_logit: float32 [16], P('tp'), may hold values from 2 to 6
- conv_taps: float32 [31, 1024], P(None, 'tp'), may hold values from -5.3881591 to 5.3881591
- conv_bias: float32 [1024], P('tp'), may hold values from -0.9 to 5.9
- channel_gain: float32 [1024], P('tp'), may hold values from 0.1 to 1.9
- channel_shift: float32 [1024], P('tp'), may hold values from -3 to 3
- w_attn_out: bfloat16 [1024, 2048], P(None, 'sp'), may hold values from -1.5 to 1.5
- w_conv_out: bfloat16 [1024, 2048], P(None, 'sp'), may hold values from -0.1875 to 0.1875
Outputs:
- output: bfloat16 [4096, 2048], P(('fs', 'sp', 'tp')), parts along dimension 0
There are 4 independent parts, one for each index of `fs`. A program takes and returns all parts, laid end to end along the dimension named above; an argument that names none is the same for every part. Nothing has to cross between parts.
All inputs are finite; a program needn't handle non-finite values.
Results may differ from a plain program's by a relative error of at most 0.011.
Values may be sent and summed in bfloat16 or wider, within the bound.
A program may use at most 64 MiB of HBM per device.

v0:
```python
import jax
import jax.numpy as jnp
from jax import lax
from jax.sharding import PartitionSpec as P

HEAD_DIM = 64
WINDOW = 128
GRID_W = 64


EPSILON = 1e-06
NEGATIVE = -1e30
ROPE_BASE = 10000.0


def padded(block, sides, width):
    for axis, dim in sides:
        count = lax.axis_size(axis)
        forward = [(i, i + 1) for i in range(count - 1)]
        backward = [(target, source) for source, target in forward]
        low = lax.ppermute(
            lax.slice_in_dim(block, block.shape[dim] - width, None, axis=dim), axis, forward
        )
        high = lax.ppermute(lax.slice_in_dim(block, 0, width, axis=dim), axis, backward)
        block = jnp.concatenate([low, block, high], axis=dim)
    return block


def rotate_pairs(values, positions):
    middle = values.shape[-1] // 2
    inverse = ROPE_BASE ** (-jnp.arange(middle, dtype=jnp.float32) / middle)
    angles = positions.astype(jnp.float32)[:, None] * inverse[None, :]
    cosine = jnp.cos(angles)[:, None, :]
    sine_table = jnp.sin(angles)[:, None, :]
    leading = values[..., :middle]
    trailing = values[..., middle:]
    return jnp.concatenate(
        [leading * cosine - trailing * sine_table, leading * sine_table + trailing * cosine],
        axis=-1,
    )


def grid_rotate(values, positions):
    middle = values.shape[-1] // 2
    return jnp.concatenate(
        [
            rotate_pairs(values[..., :middle], positions // GRID_W),
            rotate_pairs(values[..., middle:], positions % GRID_W),
        ],
        axis=-1,
    )


def local(
    tokens,
    norm_gain,
    w_query,
    w_key,
    w_value,
    w_conv_in,
    w_conv_gate,
    sink_logit,
    conv_taps,
    conv_bias,
    channel_gain,
    channel_shift,
    w_attn_out,
    w_conv_out,
):
    rows_here = tokens.shape[0]
    offset = lax.axis_index("sp") * rows_here
    total = rows_here * lax.axis_size("sp")
    tp_count = lax.axis_size("tp")
    token_float = tokens.astype(jnp.float32)
    normed = (
        token_float
        * lax.rsqrt(jnp.mean(token_float * token_float, axis=-1, keepdims=True) + EPSILON)
        * norm_gain[None, :]
    ).astype(jnp.bfloat16)
    head_cols = w_query.shape[1]
    kv_cols = w_key.shape[1]
    chan_cols = w_conv_in.shape[1]
    piece_query = lax.all_gather(w_query, "sp", axis=0, tiled=True)
    piece_key = lax.all_gather(w_key, "sp", axis=0, tiled=True)
    piece_value = lax.all_gather(w_value, "sp", axis=0, tiled=True)
    piece_conv = lax.all_gather(w_conv_in, "sp", axis=0, tiled=True)
    piece_gate = lax.all_gather(w_conv_gate, "sp", axis=0, tiled=True)
    query_acc = jnp.dot(normed, piece_query, preferred_element_type=jnp.float32)
    pair_acc = jnp.dot(
        normed,
        jnp.concatenate([piece_key, piece_value], axis=1),
        preferred_element_type=jnp.float32,
    )
    conv_acc = jnp.dot(
        normed,
        jnp.concatenate([piece_conv, piece_gate], axis=1),
        preferred_element_type=jnp.float32,
    )
    positions = offset + jnp.arange(rows_here, dtype=jnp.int32)
    heads_here = head_cols // HEAD_DIM
    kv_here = kv_cols // HEAD_DIM
    group = heads_here // kv_here
    query = grid_rotate(query_acc.reshape(rows_here, heads_here, HEAD_DIM), positions).astype(
        jnp.bfloat16
    )
    keys = grid_rotate(pair_acc[:, :kv_cols].reshape(rows_here, kv_here, HEAD_DIM), positions)
    keys = keys.astype(jnp.bfloat16).reshape(rows_here, kv_cols)
    values = pair_acc[:, kv_cols:].astype(jnp.bfloat16)
    stacked = jnp.concatenate([keys, values], axis=1)
    extended = padded(stacked, (("sp", 0),), WINDOW)
    block = min(rows_here, 512)
    span = block + 2 * WINDOW
    sinks = sink_logit.reshape(kv_here, group)[:, :, None, None]
    queries = query.reshape(block, kv_here, group, HEAD_DIM)
    near_keys = extended[:, :kv_cols].reshape(span, kv_here, HEAD_DIM)
    near_values = extended[:, kv_cols:].reshape(span, kv_here, HEAD_DIM)
    scores = jnp.einsum(
        "qkgd,skd->kgqs", queries, near_keys, preferred_element_type=jnp.float32
    ) * HEAD_DIM ** (-0.5)
    query_pos = offset + 0 + jnp.arange(block, dtype=jnp.int32)
    key_pos = offset + 0 - WINDOW + jnp.arange(span, dtype=jnp.int32)
    valid = (
        (jnp.abs(query_pos[:, None] - key_pos[None, :]) <= WINDOW)
        & (key_pos[None, :] >= 0)
        & (key_pos[None, :] < total)
    )
    scores = jnp.where(valid[None, None], scores, NEGATIVE)
    top = jnp.maximum(jnp.max(scores, axis=-1, keepdims=True), sinks)
    raised = jnp.exp(scores - top)
    denominator = jnp.sum(raised, axis=-1, keepdims=True) + jnp.exp(sinks - top)
    probs = (raised / denominator).astype(jnp.bfloat16)
    mixed = jnp.einsum("kgqs,skd->qkgd", probs, near_values, preferred_element_type=jnp.float32)
    outputs = mixed.astype(jnp.bfloat16).reshape(block, head_cols)
    glu = (conv_acc[:, :chan_cols] * jax.nn.sigmoid(conv_acc[:, chan_cols:])).astype(jnp.bfloat16)
    reach = conv_taps.shape[0] // 2
    rims = padded(glu, (("sp", 0),), reach)
    filtered = jnp.zeros((rows_here, chan_cols), jnp.float32) + conv_bias[None, :]
    for shift_index in range(conv_taps.shape[0]):
        filtered = filtered + conv_taps[shift_index][None, :] * rims[
            shift_index : shift_index + rows_here
        ].astype(jnp.float32)
    channel_total = chan_cols * tp_count
    centre = lax.psum(jnp.sum(filtered, axis=-1), "tp")[:, None] / channel_total
    centred = filtered - centre
    spread = lax.psum(jnp.sum(centred * centred, axis=-1), "tp")[:, None] / channel_total
    conv_out = jax.nn.silu(
        centred * lax.rsqrt(spread + EPSILON) * channel_gain[None, :] + channel_shift[None, :]
    ).astype(jnp.bfloat16)
    features = jnp.concatenate([outputs, conv_out], axis=1)
    tp_here = lax.axis_index("tp")
    own_rows = jnp.concatenate(
        [
            lax.dynamic_slice_in_dim(w_attn_out, tp_here * head_cols, head_cols, 0),
            lax.dynamic_slice_in_dim(w_conv_out, tp_here * chan_cols, chan_cols, 0),
        ],
        axis=0,
    )
    own_whole = lax.all_gather(own_rows, "sp", axis=1, tiled=True)
    result = lax.psum_scatter(
        jnp.dot(features, own_whole, preferred_element_type=jnp.float32).astype(jnp.bfloat16),
        "tp",
        scatter_dimension=0,
        tiled=True,
    )
    return result


def solution(mesh):
    in_specs = (
        P(("fs", "sp"), None),
        P(),
        P("sp", "tp"),
        P("sp", "tp"),
        P("sp", "tp"),
        P("sp", "tp"),
        P("sp", "tp"),
        P("tp"),
        P(None, "tp"),
        P("tp"),
        P("tp"),
        P("tp"),
        P(None, "sp"),
        P(None, "sp"),
    )
    out_specs = P(("fs", "sp", "tp"), None)
    return jax.shard_map(local, mesh=mesh, in_specs=in_specs, out_specs=out_specs, check_vma=False)
```

profile of v0, /device:TPU:0, one launch (start us, length us, event | category | flops | bytes accessed | tf_op | source)
XLA Modules:
  0.0 263.5 jit_solution(13735289390232705822)
XLA Ops:
  6.5 0.7 all-gather.7.cloned.1.call-update
  7.3 0.0 all-gather.9.cloned.1.call-start
  7.3 0.7 all-gather.9.cloned.1.call-update
  8.0 0.0 all-gather.5.cloned.1.call-start
  8.1 0.7 all-gather.5.cloned.1.call-update
  8.8 0.0 all-gather.11.cloned.1.call-start
  8.8 1.3 constant_dynamic-slice_fusion
  10.1 1.0 pad_maximum_fusion
  11.1 0.0 all-gather.11.cloned.1.call-update
  11.2 0.0 reduce-scatter.2.cloned.1.call-start
  11.3 0.3 fusion.6
  11.6 23.1 %all_gather.18 = bf16[2048,128]{1,0:T(8,128)(2,1)S(1)} all-gather(bf16[512,128]{1,0:T(8,128)(2,1)S(1)} %copy-done.1), channel_id=1, replica_groups=mesh['sp'=4,'fs'=4,'tp'=2] {'sp'}, dimensions={0}, use_global_device_ids=true | all-gather | bytes 655360 | tf_op jit(solution)/shard_map/all_gather | solution.py:84
  34.7 21.7 %all_gather.19 = bf16[2048,128]{1,0:T(8,128)(2,1)S(1)} all-gather(bf16[512,128]{1,0:T(8,128)(2,1)S(1)} %copy-done.2), channel_id=1, replica_groups=mesh['sp'=4,'fs'=4,'tp'=2] {'sp'}, dimensions={0}, use_global_device_ids=true | all-gather | bytes 655360 | tf_op jit(solution)/shard_map/all_gather | solution.py:85
  56.4 0.7 fusion.11
  57.1 0.2 multiply_cosine_fusion.1
  57.4 1.5 collective-permute-start
  58.9 1.3 collective-permute-start.1
  60.3 0.3 fusion.24
  60.6 0.1 max.18
  60.7 1.5 collective-permute-done
  62.2 7.0 %collective-permute-done.1 = bf16[128,256]{0,1:T(8,128)(2,1)S(1)} collective-permute-done((bf16[128,256]{0,1:T(8,128)(2,1)S(1)}, bf16[128,256]{0,1:T(8,128)(2,1)S(1)}, u32[]{:S(2)}, u32[]{:S(2)}) %collective-permute-start.1) | collective-permute-done | bytes 65568 | tf_op jit(solution)/shard_map/ppermute | solution.py:24
  69.2 1.9 all-gather.7.cloned.1.call-done
  71.1 47.3 %all-gather.9.cloned.1.call-done = bf16[2048,512]{1,0:T(8,128)(2,1)} async-done(((bf16[512,512]{1,0:T(8,128)(2,1)}), bf16[2048,512]{1,0:T(8,128)(2,1)}) %all-gather.9.cloned.1.call-update) | async-done | bytes 2097168 | tf_op jit(solution)/shard_map/all_gather | solution.py:87
  118.4 3.5 %fusion = f32[256,1024]{1,0:T(8,128)S(1)} fusion(bf16[2048,512]{1,0:T(8,128)(2,1)} %all-gather.9.cloned.1.call-done, bf16[2048,512]{1,0:T(8,128)(2,1)} %all-gather.7.cloned.1.call-done, bf16[256,2048]{1,0:T(8,128)(2,1)S(1)} %copy-done, f32[2048]{0:T(1024)S(1)} %copy-done.7, f32[256]{0:T(256)S(1)} %add_rsqrt_fusion.1), kind=kOutput, calls=%fused_computation | convolution fusion | flops 1084227584 | bytes 6300672 | tf_op jit(solution)/shard_map/dot_general | solution.py:94
  121.9 0.1 fusion.22
  122.1 2.1 collective-permute-start.2
  124.2 1.3 collective-permute-start.3
  125.5 39.2 %all-gather.5.cloned.1.call-done = bf16[2048,512]{1,0:T(8,128)(2,1)} async-done(((bf16[512,512]{1,0:T(8,128)(2,1)}), bf16[2048,512]{1,0:T(8,128)(2,1)}) %all-gather.5.cloned.1.call-update) | async-done | bytes 2097168 | tf_op jit(solution)/shard_map/all_gather | solution.py:83
  164.6 2.6 fusion.74
  167.2 0.1 subtract_convert_fusion.1
  167.3 0.8 fusion.5
  168.2 0.1 broadcast_maximum_fusion
  168.2 0.9 fusion.4
  169.1 0.1 exponential_add_fusion
  169.2 0.0 copy-start.4
  169.2 0.0 copy-start.5
  169.2 0.0 copy-start.6
  169.3 1.2 fusion.10
  170.5 0.1 copy.27
  170.7 3.1 %fusion.77 = (f32[256]{0:T(256)S(1)}, f32[256,512]{1,0:T(8,128)S(1)}) fusion(bf16[15,512]{1,0:T(8,128)(2,1)S(1)} %collective-permute-done.3, bf16[256,512]{1,0:T(8,128)(2,1)S(1)} %fusion.22, f32[512]{0:T(512)S(1)} %bitcast.106, f32[512]{0:T(512)S(1)} %bitcast.107, f32[512]{0:T(512)S(1)} %bitcast.78, f32[512]{0:T(512)S(1)} %bitcast.79, f32[512]{0:T(512)S(1)} %bitcast.80, ...), kind=kLoop, calls=%fused_computation.167 | loop fusion | flops 24116992 | bytes 883712 | tf_op jit(solution)/shard_map/reduce_sum | solution.py:143
  173.8 2.5 psum.14
  176.2 0.2 multiply_reduce_fusion
  176.4 2.5 psum.15
  178.9 0.3 multiply_convert_fusion
  179.2 66.3 %all-gather.11.cloned.1.call-done = bf16[1024,2048]{1,0:T(8,128)(2,1)} async-done(((bf16[1024,512]{1,0:T(8,128)(2,1)}), bf16[1024,2048]{1,0:T(8,128)(2,1)}) %all-gather.11.cloned.1.call-update) | async-done | bytes 4194320 | tf_op jit(solution)/shard_map/all_gather | solution.py:158
  245.5 4.5 %convolution_convert_fusion = bf16[256,2048]{1,0:T(8,128)(2,1)} fusion(bf16[1024,2048]{1,0:T(8,128)(2,1)} %all-gather.11.cloned.1.call-done, bf16[256,512]{1,0:T(8,128)(2,1)S(1)} %multiply_convert_fusion, bf16[256,512]{1,0:T(8,128)(2,1)S(1)} %copy.27), kind=kOutput, calls=%fused_computation.11 | convolution fusion | flops 1075314688 | bytes 5767168 | tf_op jit(solution)/shard_map/dot_general | solution.py:160
  249.9 0.0 reduce-scatter.2.cloned.1.call-update
  249.9 7.0 %reduce-scatter.2.cloned.1.call-done = bf16[128,2048]{1,0:T(8,128)(2,1)} async-done(((bf16[256,2048]{1,0:T(8,128)(2,1)}), bf16[128,2048]{1,0:T(8,128)(2,1)}) %reduce-scatter.2.cloned.1.call-update) | async-done | bytes 524304 | tf_op jit(solution)/shard_map/reduce_scatter | solution.py:159
  (36 shorter events, 0.3 us)
Async XLA Ops:
  6.5 4.7 %copy-start = (bf16[256,2048]{1,0:T(8,128)(2,1)S(1)}, bf16[256,2048]{1,0:T(8,128)(2,1)}, u32[]{:S(2)}) copy-start(bf16[256,2048]{1,0:T(8,128)(2,1)} %param.14) | copy-start | bytes 3145732
  6.5 5.0 %copy-start.1 = (bf16[512,128]{1,0:T(8,128)(2,1)S(1)}, bf16[512,128]{1,0:T(8,128)(2,1)}, u32[]{:S(2)}) copy-start(bf16[512,128]{1,0:T(8,128)(2,1)} %param.17) | copy-start | bytes 393220
  6.5 28.1 %copy-start.2 = (bf16[512,128]{1,0:T(8,128)(2,1)S(1)}, bf16[512,128]{1,0:T(8,128)(2,1)}, u32[]{:S(2)}) copy-start(bf16[512,128]{1,0:T(8,128)(2,1)} %param.18) | copy-start | bytes 393220
  6.5 64.6 %all-gather.7.cloned.1.call-start = ((), (), s32[]{:S(2)}) async-start(), calls=%async_computation.2 | async-start | bytes 2621440 | tf_op jit(solution)/shard_map/all_gather | solution.py:86
  7.3 111.1 %all-gather.9.cloned.1.call-start = ((), (), s32[]{:S(2)}) async-start(), calls=%async_computation.3 | async-start | bytes 2621440 | tf_op jit(solution)/shard_map/all_gather | solution.py:87
  8.0 48.4 %copy-start.7 = (f32[2048]{0:T(1024)S(1)}, f32[2048]{0:T(1024)}, u32[]{:S(2)}) copy-start(f32[2048]{0:T(1024)} %param.15) | copy-start | bytes 24580
  8.0 156.6 %all-gather.5.cloned.1.call-start = ((), (), s32[]{:S(2)}) async-start(), calls=%async_computation.1 | async-start | bytes 2621440 | tf_op jit(solution)/shard_map/all_gather | solution.py:83
  8.8 236.7 %all-gather.11.cloned.1.call-start = ((), (), s32[]{:S(2)}) async-start(), calls=%async_computation.4 | async-start | bytes 5242880 | tf_op jit(solution)/shard_map/all_gather | solution.py:158
  11.1 49.1 %copy-start.3 = (f32[31,512]{1,0:T(8,128)S(1)}, f32[31,512]{1,0:T(8,128)}, u32[]{:S(2)}) copy-start(f32[31,512]{1,0:T(8,128)} %param.22) | copy-start | bytes 190468
  11.1 49.5 %copy-start.8 = (f32[8]{0:T(128)S(1)}, f32[8]{0:T(128)}, u32[]{:S(2)}) copy-start(f32[8]{0:T(128)} %param.21) | copy-start | bytes 100
  11.2 245.8 %reduce-scatter.2.cloned.1.call-start = ((), (), s32[]{:S(2)}) async-start(), calls=%async_computation.5 | async-start | bytes 1572864 | tf_op jit(solution)/shard_map/reduce_scatter | solution.py:159
  57.4 4.8 %collective-permute-start = (bf16[128,256]{0,1:T(8,128)(2,1)S(1)}, bf16[128,256]{0,1:T(8,128)(2,1)S(1)}, u32[]{:S(2)}, u32[]{:S(2)}) collective-permute-start(bf16[128,256]{0,1:T(8,128)(2,1)S(1)} %get-tuple-element.21), channel_id=1, source_target_pairs={{0,8},{8,16},{16,24},{1,9},{9,17},{17,25},{2,10},{10,18},{18,26},{... | collective-permute-start | bytes 196616 | tf_op jit(solution)/shard_map/ppermute | solution.py:21
  58.9 10.3 %collective-permute-start.1 = (bf16[128,256]{0,1:T(8,128)(2,1)S(1)}, bf16[128,256]{0,1:T(8,128)(2,1)S(1)}, u32[]{:S(2)}, u32[]{:S(2)}) collective-permute-start(bf16[128,256]{0,1:T(8,128)(2,1)S(1)} %get-tuple-element.22), channel_id=1, source_target_pairs={{8,0},{16,8},{24,16},{9,1},{17,9},{25,17},{10,2},{18,10},{26,18},{... | collective-permute-start | bytes 196616 | tf_op jit(solution)/shard_map/ppermute | solution.py:24
  122.1 48.6 %collective-permute-start.2 = (bf16[15,512]{1,0:T(8,128)(2,1)S(1)}, bf16[15,512]{1,0:T(8,128)(2,1)S(1)}, u32[]{:S(2)}, u32[]{:S(2)}) collective-permute-start(bf16[15,512]{1,0:T(8,128)(2,1)S(1)} %get-tuple-element.15), channel_id=1, source_target_pairs={{0,8},{8,16},{16,24},{1,9},{9,17},{17,25},{2,10},{10,18},{18,26},{... | collective-permute-start | bytes 46088 | tf_op jit(solution)/shard_map/ppermute | solution.py:21
  124.2 46.5 %collective-permute-start.3 = (bf16[15,512]{1,0:T(8,128)(2,1)S(1)}, bf16[15,512]{1,0:T(8,128)(2,1)S(1)}, u32[]{:S(2)}, u32[]{:S(2)}) collective-permute-start(bf16[15,512]{1,0:T(8,128)(2,1)S(1)} %get-tuple-element.16), channel_id=1, source_target_pairs={{8,0},{16,8},{24,16},{9,1},{17,9},{25,17},{10,2},{18,10},{26,18},{... | collective-permute-start | bytes 46088 | tf_op jit(solution)/shard_map/ppermute | solution.py:24
  169.2 1.4 copy-start.4
  169.2 9.7 %copy-start.5 = (f32[512]{0:T(512)S(1)}, f32[512]{0:T(512)}, u32[]{:S(2)}) copy-start(f32[512]{0:T(512)} %param.25) | copy-start | bytes 6148
  169.2 9.7 %copy-start.6 = (f32[512]{0:T(512)S(1)}, f32[512]{0:T(512)}, u32[]{:S(2)}) copy-start(f32[512]{0:T(512)} %param.24) | copy-start | bytes 6148
Sparse Core Ops, SparseCore 0:
  8.9 62.1 all-gather.6
  72.7 45.6 all-gather.8
  120.0 44.6 all-gather.4
  166.1 79.3 all-gather.10
  250.1 6.8 reduce-scatter.1
where the time goes:
time: 264 us
  waiting for transfers between devices  172 us (65%)
  blocking collectives  49.7 us (19%)
  between operations  13.5 us (5%)
  matrix products  13.3 us (5%)
  other arithmetic  6.78 us (3%)
  starting transfers between devices  6.35 us (2%)
    all_gather x1, waiting for transfers between devices, local(): own_whole = lax.all_gather(own_rows, 'sp', axis=1, tiled=True)  66.3 us
    all_gather x1, waiting for transfers between devices, local(): piece_gate = lax.all_gather(w_conv_gate, 'sp', axis=0, tiled=True)  47.3 us
    all_gather x1, waiting for transfers between devices, local(): piece_query = lax.all_gather(w_query, 'sp', axis=0, tiled=True)  39.2 us
    all_gather x1, blocking collectives, local(): piece_key = lax.all_gather(w_key, 'sp', axis=0, tiled=True)  23.1 us
    all_gather x1, blocking collectives, local(): piece_value = lax.all_gather(w_value, 'sp', axis=0, tiled=True)  21.7 us
    reduce_scatter x1, waiting for transfers between devices, local(): lax.psum_scatter(jnp.dot(features, own_whole, preferred_element_type=jnp....  7.04 us
    ppermute x2, waiting for transfers between devices, padded(): lax.ppermute(lax.slice_in_dim(block, 0, width, axis=dim), axis, backward)  6.99 us
  transfers between devices with their start and end apart: 9, of which 7 were waited for; matrix products, arithmetic and copies ran while one was open for 7% of the time, Pallas kernels for 0%

commit v1 on v0

v1 whole, which is shorter than its diff:
```python
import jax
import jax.numpy as jnp
from jax import lax
from jax.sharding import PartitionSpec as P

HEAD_DIM = 64
WINDOW = 128
GRID_W = 64


EPSILON = 1e-06
NEGATIVE = -1e30
ROPE_BASE = 10000.0


def padded(block, sides, width):
    for axis, dim in sides:
        count = lax.axis_size(axis)
        forward = [(i, i + 1) for i in range(count - 1)]
        backward = [(target, source) for source, target in forward]
        low = lax.ppermute(
            lax.slice_in_dim(block, block.shape[dim] - width, None, axis=dim), axis, forward
        )
        high = lax.ppermute(lax.slice_in_dim(block, 0, width, axis=dim), axis, backward)
        block = jnp.concatenate([low, block, high], axis=dim)
    return block


def rotate_pairs(values, positions):
    middle = values.shape[-1] // 2
    inverse = ROPE_BASE ** (-jnp.arange(middle, dtype=jnp.float32) / middle)
    angles = positions.astype(jnp.float32)[:, None] * inverse[None, :]
    cosine = jnp.cos(angles)[:, None, :]
    sine_table = jnp.sin(angles)[:, None, :]
    leading = values[..., :middle]
    trailing = values[..., middle:]
    return jnp.concatenate(
        [leading * cosine - trailing * sine_table, leading * sine_table + trailing * cosine],
        axis=-1,
    )


def grid_rotate(values, positions):
    middle = values.shape[-1] // 2
    return jnp.concatenate(
        [
            rotate_pairs(values[..., :middle], positions // GRID_W),
            rotate_pairs(values[..., middle:], positions % GRID_W),
        ],
        axis=-1,
    )


def gather_inputs(normed, packed_in):
    return (
        lax.all_gather(normed, ("fs", "tp"), axis=0, tiled=True),
        lax.all_gather(packed_in, "sp", axis=0, tiled=True),
    )


def gather_outputs(packed_out, after):
    return lax.all_gather(packed_out, "sp", axis=1, tiled=True)


def gather_stats(pair):
    return lax.all_gather(pair, ("fs", "tp"), axis=0)


def scatter_sum(features, whole_out):
    partial = jnp.dot(features, whole_out, preferred_element_type=jnp.float32)
    return lax.psum_scatter(
        partial.astype(jnp.bfloat16), ("fs", "tp"), scatter_dimension=0, tiled=True
    )


def local(
    tokens,
    norm_gain,
    w_query,
    w_key,
    w_value,
    w_conv_in,
    w_conv_gate,
    sink_logit,
    conv_taps,
    conv_bias,
    channel_gain,
    channel_shift,
    w_attn_out,
    w_conv_out,
):
    rows_here = tokens.shape[0]
    sp_count = lax.axis_size("sp")
    fs_count = lax.axis_size("fs")
    tp_count = lax.axis_size("tp")
    sp_here = lax.axis_index("sp")
    fs_here = lax.axis_index("fs")
    tp_here = lax.axis_index("tp")
    offset = sp_here * rows_here
    total = rows_here * sp_count
    head_tp = w_query.shape[1]
    chan_tp = w_conv_in.shape[1]
    head_cols = head_tp // fs_count
    chan_cols = chan_tp // fs_count
    heads_here = head_cols // HEAD_DIM
    kv_tp = w_key.shape[1] // HEAD_DIM
    group = (head_tp // HEAD_DIM) // kv_tp
    kv_here = max(1, kv_tp // fs_count)
    kv_cols = kv_here * HEAD_DIM
    group_here = heads_here // kv_here
    head_at = fs_here * heads_here
    kv_at = (head_at // group) * HEAD_DIM

    def columns(array, start, size, axis=-1):
        return lax.dynamic_slice_in_dim(array, start, size, axis % array.ndim)

    half = rows_here // tp_count
    token_float = columns(tokens, tp_here * half, half, 0).astype(jnp.float32)
    normed = (
        token_float
        * lax.rsqrt(jnp.mean(token_float * token_float, axis=-1, keepdims=True) + EPSILON)
        * norm_gain[None, :]
    ).astype(jnp.bfloat16)
    packed_in = jnp.concatenate(
        [
            columns(w_query, fs_here * head_cols, head_cols),
            columns(w_conv_in, fs_here * chan_cols, chan_cols),
            columns(w_conv_gate, fs_here * chan_cols, chan_cols),
            columns(w_key, kv_at, kv_cols),
            columns(w_value, kv_at, kv_cols),
        ],
        axis=1,
    )
    packed_out = jnp.concatenate(
        [
            columns(w_attn_out, tp_here * head_tp + fs_here * head_cols, head_cols, 0),
            columns(w_conv_out, tp_here * chan_tp + fs_here * chan_cols, chan_cols, 0),
        ],
        axis=0,
    )
    whole_normed, whole_in = gather_inputs(normed, packed_in)
    whole_out = gather_outputs(packed_out, whole_in)
    acc = jnp.dot(whole_normed, whole_in, preferred_element_type=jnp.float32)
    cut = [head_cols, head_cols + chan_cols, head_cols + 2 * chan_cols]
    cut.append(cut[2] + kv_cols)
    tokens_here = fs_count * rows_here
    positions = offset + jnp.arange(tokens_here, dtype=jnp.int32) % rows_here
    query = grid_rotate(acc[:, : cut[0]].reshape(tokens_here, heads_here, HEAD_DIM), positions)
    keys = grid_rotate(acc[:, cut[2] : cut[3]].reshape(tokens_here, kv_here, HEAD_DIM), positions)
    query = query.astype(jnp.bfloat16)
    keys = keys.astype(jnp.bfloat16).reshape(fs_count, rows_here, kv_cols)
    values = acc[:, cut[3] :].astype(jnp.bfloat16).reshape(fs_count, rows_here, kv_cols)
    glu = (acc[:, cut[0] : cut[1]] * jax.nn.sigmoid(acc[:, cut[1] : cut[2]])).astype(jnp.bfloat16)
    glu = glu.reshape(fs_count, rows_here, chan_cols)
    reach = conv_taps.shape[0] // 2
    rims = padded(glu, (("sp", 1),), reach)
    extended = padded(jnp.concatenate([keys, values], axis=2), (("sp", 1),), WINDOW)
    taps = columns(conv_taps, fs_here * chan_cols, chan_cols)
    bias = columns(conv_bias, fs_here * chan_cols, chan_cols)
    gain = columns(channel_gain, fs_here * chan_cols, chan_cols)
    shift = columns(channel_shift, fs_here * chan_cols, chan_cols)
    filtered = jnp.zeros((fs_count, rows_here, chan_cols), jnp.float32) + bias
    for shift_index in range(conv_taps.shape[0]):
        filtered = filtered + taps[shift_index] * rims[
            :, shift_index : shift_index + rows_here
        ].astype(jnp.float32)
    own_mean = jnp.mean(filtered, axis=-1)
    own_centred = filtered - own_mean[..., None]
    own_square = jnp.sum(own_centred * own_centred, axis=-1)
    pairs = gather_stats(
        jnp.stack([own_mean.reshape(tokens_here), own_square.reshape(tokens_here)])
    )
    centre = jnp.mean(pairs[:, 0], axis=0)
    drift = pairs[:, 0] - centre[None]
    spread = jnp.sum(pairs[:, 1] + chan_cols * (drift * drift), axis=0) / (
        chan_cols * fs_count * tp_count
    )
    centre = centre.reshape(fs_count, rows_here, 1)
    spread = spread.reshape(fs_count, rows_here, 1)

    sinks = columns(sink_logit, head_at, heads_here).reshape(kv_here, group_here)
    sinks = sinks[None, :, :, None, None]
    span = rows_here + 2 * WINDOW
    queries = query.reshape(fs_count, rows_here, kv_here, group_here, HEAD_DIM)
    near_keys = extended[..., :kv_cols].reshape(fs_count, span, kv_here, HEAD_DIM)
    near_values = extended[..., kv_cols:].reshape(fs_count, span, kv_here, HEAD_DIM)
    scores = jnp.einsum(
        "bqkgd,bskd->bkgqs", queries, near_keys, preferred_element_type=jnp.float32
    ) * HEAD_DIM ** (-0.5)
    query_pos = offset + jnp.arange(rows_here, dtype=jnp.int32)
    key_pos = offset - WINDOW + jnp.arange(span, dtype=jnp.int32)
    valid = (
        (jnp.abs(query_pos[:, None] - key_pos[None, :]) <= WINDOW)
        & (key_pos[None, :] >= 0)
        & (key_pos[None, :] < total)
    )
    scores = jnp.where(valid, scores, NEGATIVE)
    top = jnp.maximum(jnp.max(scores, axis=-1, keepdims=True), sinks)
    raised = jnp.exp(scores - top)
    denominator = jnp.sum(raised, axis=-1, keepdims=True) + jnp.exp(sinks - top)
    probs = (raised / denominator).astype(jnp.bfloat16)
    mixed = jnp.einsum("bkgqs,bskd->bqkgd", probs, near_values, preferred_element_type=jnp.float32)
    attended = mixed.astype(jnp.bfloat16).reshape(tokens_here, head_cols)
    conv_out = jax.nn.silu(
        (filtered - centre) * lax.rsqrt(spread + EPSILON) * gain + shift
    ).astype(jnp.bfloat16)
    features = jnp.concatenate([attended, conv_out.reshape(tokens_here, chan_cols)], axis=1)
    return scatter_sum(features, whole_out)


def solution(mesh):
    in_specs = (
        P(("fs", "sp"), None),
        P(),
        P("sp", "tp"),
        P("sp", "tp"),
        P("sp", "tp"),
        P("sp", "tp"),
        P("sp", "tp"),
        P("tp"),
        P(None, "tp"),
        P("tp"),
        P("tp"),
        P("tp"),
        P(None, "sp"),
        P(None, "sp"),
    )
    out_specs = P(("fs", "sp", "tp"), None)
    return jax.shard_map(local, mesh=mesh, in_specs=in_specs, out_specs=out_specs, check_vma=False)
```

time: 264 us -> 214 us (0.81)
  blocking collectives: 49.7 us -> 9.4 us
  waiting for transfers between devices: 172 us -> 138 us
  other arithmetic: 6.78 us -> 18.2 us
  local copies, waits for them, and re-layouts: 1.64 us -> 10.7 us
  starting transfers between devices: 6.35 us -> 11.3 us
    all_gather x4 -> x3, waiting for transfers between devices: 155 us -> 75.2 us  [the longest x1 37.9 us: gather_inputs(): lax.all_gather(packed_in, 'sp', axis=0, tiled=True)]
    reduce_scatter x1, waiting for transfers between devices: 7.04 us -> 48.8 us  [scatter_sum(): lax.psum_scatter(partial.astype(jnp.bfloat16), ('fs', 'tp'), scatter_dime...]
    all_gather x2 -> x1, blocking collectives: 44.8 us -> 9.4 us  [gather_stats(): return lax.all_gather(pair, ('fs', 'tp'), axis=0)]
    reduce_sum x2 -> x4, other arithmetic: 3.28 us -> 11 us  [the longest x1 10.7 us: local(): own_mean = jnp.mean(filtered, axis=-1)]
    ppermute x2, waiting for transfers between devices: 6.99 us -> 14.2 us  [padded(): lax.ppermute(lax.slice_in_dim(block, 0, width, axis=dim), axis, backward)]
    ppermute x2, starting transfers between devices: 3.61 us -> 8.58 us  [padded(): lax.ppermute(lax.slice_in_dim(block, block.shape[dim] - width, None, axis...]
    psum x2 -> x0, blocking collectives: 4.94 us -> none  [the longest x1 2.47 us: local(): centre = lax.psum(jnp.sum(filtered, axis=-1), 'tp')[:, None] / channel_total]
    dynamic_slice x1 -> x8, local copies, waits for them, and re-layouts: 1.27 us -> 5.46 us  [columns(): return lax.dynamic_slice_in_dim(array, start, size, axis % array.ndim)]
  transfers between devices with their start and end apart: 9 -> 8, of which waited for: 7 -> 4; matrix products, arithmetic and copies ran while one was open for 7% -> 15% of each run, Pallas kernels for 0% -> 0%
where the time goes in v1:
time: 214 us; the launch traced here: 213 us
  waiting for transfers between devices  138 us (64%)
  other arithmetic  18.2 us (9%)
  between operations  13.6 us (6%)
  matrix products  11.8 us (6%)
  starting transfers between devices  11.3 us (5%)
  local copies, waits for them, and re-layouts  10.7 us (5%)
  blocking collectives  9.4 us (4%)
    reduce_scatter x1, waiting for transfers between devices, scatter_sum(): lax.psum_scatter(partial.astype(jnp.bfloat16), ('fs', 'tp'), scatter_dime...  48.8 us
    all_gather x1, waiting for transfers between devices, gather_inputs(): lax.all_gather(packed_in, 'sp', axis=0, tiled=True)  37.9 us
    all_gather x1, waiting for transfers between devices, gather_inputs(): lax.all_gather(normed, ('fs', 'tp'), axis=0, tiled=True)  37.3 us
    ppermute x2, waiting for transfers between devices, padded(): lax.ppermute(lax.slice_in_dim(block, 0, width, axis=dim), axis, backward)  14.2 us
    reduce_sum x1, other arithmetic, local(): own_mean = jnp.mean(filtered, axis=-1)  10.7 us
    all_gather x1, blocking collectives, gather_stats(): return lax.all_gather(pair, ('fs', 'tp'), axis=0)  9.4 us
    ppermute x2, starting transfers between devices, padded(): lax.ppermute(lax.slice_in_dim(block, block.shape[dim] - width, None, axis...  8.58 us
    dynamic_slice x8, local copies, waits for them, and re-layouts, columns(): return lax.dynamic_slice_in_dim(array, start, size, axis % array.ndim)  5.46 us
  transfers between devices with their start and end apart: 8, of which 4 were waited for; matrix products, arithmetic and copies ran while one was open for 15% of the time, Pallas kernels for 0%

profile of v1, /device:TPU:0, one launch (start us, length us, event | category | flops | bytes accessed | tf_op | source)
XLA Modules:
  0.0 213.2 jit_solution(7359551569664996277)
XLA Ops:
  6.5 1.0 copy-done
  7.6 1.0 constant_dynamic-slice_fusion.5
  8.6 1.1 constant_dynamic-slice_fusion.3
  9.7 1.0 concatenate.78
  10.7 0.0 all-gather.6.cloned.1.call-start
  10.8 1.2 fusion.10
  12.0 2.0 fusion.12
  14.1 0.0 all-gather.10.cloned.1.call-start
  14.2 1.0 constant_dynamic-slice_fusion.1
  15.2 0.7 pad_maximum_fusion.2
  15.9 0.0 reduce-scatter.2.cloned.1.call-start
  16.0 0.8 dynamic_slice.46
  16.8 0.8 dynamic_slice.48
  17.5 0.8 dynamic_slice.49
  18.3 0.1 dynamic_slice.45
  18.4 0.5 multiply_cosine_fusion.1
  18.9 0.3 fusion.23
  19.2 1.1 dynamic-slice_bitcast_fusion.29
  20.2 1.1 fusion.77
  21.4 37.9 %all-gather.8.cloned.1.call-done = bf16[2048,512]{1,0:T(8,128)(2,1)} async-done(((bf16[512,512]{1,0:T(8,128)(2,1)}), bf16[2048,512]{1,0:T(8,128)(2,1)}) %all-gather.8.cloned.1.call-update) | async-done | bytes 2097168 | tf_op jit(solution)/shard_map/all_gather | solution.py:57
  59.3 37.3 %all-gather.6.cloned.1.call-done = bf16[1024,2048]{1,0:T(8,128)(2,1)} async-done(((bf16[128,2048]{1,0:T(8,128)(2,1)}), bf16[1024,2048]{1,0:T(8,128)(2,1)}) %all-gather.6.cloned.1.call-update) | async-done | bytes 4194320 | tf_op jit(solution)/shard_map/all_gather | solution.py:56
  96.6 5.2 %fusion.87 = f32[1024,512]{0,1:T(8,128)S(1)} fusion(bf16[1024,2048]{1,0:T(8,128)(2,1)} %all-gather.6.cloned.1.call-done, bf16[2048,512]{1,0:T(8,128)(2,1)} %all-gather.8.cloned.1.call-done), kind=kOutput, calls=%fused_computation.206 | convolution fusion | flops 2147483648 | bytes 8388608 | tf_op jit(solution)/shard_map/dot_general | solution.py:143
  101.9 0.2 fusion.84
  102.1 0.2 reshape.443
  102.2 0.1 fusion.86
  102.4 0.1 constant_dynamic-update-slice_fusion.1
  102.5 0.6 fusion.57
  103.3 3.4 %collective-permute-start = (bf16[4,128,128]{1,2,0:T(8,128)(2,1)S(1)}, bf16[4,128,128]{1,2,0:T(8,128)(2,1)S(1)}, u32[]{:S(2)}, u32[]{:S(2)}) collective-permute-start(bf16[4,128,128]{1,2,0:T(8,128)(2,1)S(1)} %get-tuple-element.21), channel_id=1, source_target_pairs={{0,8},{8,16},{16,24},{1,9},{9,17},{17,25},{2,10},{10,18},{18,26},{... | collective-permute-start | bytes 393224 | tf_op jit(solution)/shard_map/ppermute | solution.py:21
  106.7 1.3 collective-permute-start.1
  108.0 1.3 collective-permute-start.3
  109.3 0.1 subtract_convert_fusion.1
  109.4 5.2 %collective-permute-start.2 = (bf16[4,15,128]{1,0,2:T(4,128)(2,1)S(1)}, bf16[4,15,128]{1,0,2:T(4,128)(2,1)S(1)}, u32[]{:S(2)}, u32[]{:S(2)}) collective-permute-start(bf16[4,15,128]{1,0,2:T(4,128)(2,1)S(1)} %get-tuple-element.23), channel_id=1, source_target_pairs={{0,8},{8,16},{16,24},{1,9},{9,17},{17,25},{2,10},{10,18},{18,26},{... | collective-permute-start | bytes 46088 | tf_op jit(solution)/shard_map/ppermute | solution.py:21
  114.6 14.2 %collective-permute-done.3 = bf16[4,15,128]{1,0,2:T(4,128)(2,1)S(1)} collective-permute-done((bf16[4,15,128]{1,0,2:T(4,128)(2,1)S(1)}, bf16[4,15,128]{1,0,2:T(4,128)(2,1)S(1)}, u32[]{:S(2)}, u32[]{:S(2)}) %collective-permute-start.3) | collective-permute-done | bytes 15392 | tf_op jit(solution)/shard_map/ppermute | solution.py:24
  128.8 0.1 constant_dynamic-update-slice_fusion
  128.9 10.7 %fusion.83 = (f32[4,256]{1,0:T(4,128)S(1)}, f32[4,256,128]{1,0,2:T(4,128)S(1)}) fusion(bf16[4,271,128]{1,0,2:T(4,128)(2,1)S(1)} %constant_dynamic-update-slice_fusion, f32[128]{0:T(128)S(1)} %get-tuple-element.58, f32[128]{0:T(128)S(1)} %get-tuple-element.29, f32[128]{0:T(128)S(1)} %get-tuple-element.30, f32[128]{0:T(128)S(1)} %get-tuple-element.31, ...), kind=kLoop, calls=%fused_computation.202 | loop fusion | flops 18217984 | bytes 4754432 | tf_op jit(solution)/shard_map/reduce_sum | solution.py:167
  139.7 0.2 multiply_reduce_fusion
  139.9 9.4 %all-gather.1 = f32[8,2,1024]{2,1,0:T(2,128)S(1)} all-gather(f32[1,2,1024]{2,1,0:T(2,128)S(1)} %maximum_bitcast_fusion), channel_id=2, replica_groups=mesh['sp'=4,'fs'=4,'tp'=2] {'fs','tp'}, dimensions={0}, use_global_device_ids=true | all-gather | bytes 73728 | tf_op jit(solution)/shard_map/all_gather | solution.py:66
  149.3 0.1 slice_reduce_fusion
  149.4 0.4 fusion.21
  149.9 0.1 pad_maximum_fusion
  150.0 0.8 fusion.1
  150.8 0.1 broadcast_maximum_fusion
  150.9 0.9 fusion
  151.8 0.1 exponential_add_fusion
  151.9 1.2 fusion.7
  153.1 0.2 copy.44
  153.4 4.5 %convolution_convert_fusion = bf16[1024,2048]{1,0:T(8,128)(2,1)} fusion(bf16[256,2048]{1,0:T(8,128)(2,1)} %all-gather.10.cloned.1.call-done, bf16[1024,128]{0,1:T(8,128)(2,1)S(1)} %bitcast.170, bf16[1024,128]{0,1:T(8,128)(2,1)S(1)} %bitcast.171), kind=kOutput, calls=%fused_computation.3 | convolution fusion | flops 1076887552 | bytes 5767168 | tf_op jit(solution)/shard_map/dot_general | solution.py:70
  157.9 48.8 %reduce-scatter.2.cloned.1.call-done = bf16[128,2048]{1,0:T(8,128)(2,1)} async-done(((bf16[1024,2048]{1,0:T(8,128)(2,1)}), bf16[128,2048]{1,0:T(8,128)(2,1)}) %reduce-scatter.2.cloned.1.call-update) | async-done | bytes 524304 | tf_op jit(solution)/shard_map/reduce_scatter | solution.py:71
  (46 shorter events, 0.5 us)
Async XLA Ops:
  6.5 1.0 copy-start
  6.5 11.8 %copy-start.1 = (f32[8]{0:T(128)S(1)}, f32[8]{0:T(128)}, u32[]{:S(2)}) copy-start(f32[8]{0:T(128)} %param.21) | copy-start | bytes 100
  6.5 52.7 %all-gather.8.cloned.1.call-start = ((), (), s32[]{:S(2)}) async-start(), calls=%async_computation.2 | async-start | bytes 2621440 | tf_op jit(solution)/shard_map/all_gather | solution.py:57
  10.7 85.9 %all-gather.6.cloned.1.call-start = ((), (), s32[]{:S(2)}) async-start(), calls=%async_computation.1 | async-start | bytes 4718592 | tf_op jit(solution)/shard_map/all_gather | solution.py:56
  14.1 139.3 %all-gather.10.cloned.1.call-start = ((), (), s32[]{:S(2)}) async-start(), calls=%async_computation.3 | async-start | bytes 1310720 | tf_op jit(solution)/shard_map/all_gather | solution.py:62
  15.9 190.8 %reduce-scatter.2.cloned.1.call-start = ((), (), s32[]{:S(2)}) async-start(), calls=%async_computation.4 | async-start | bytes 4718592 | tf_op jit(solution)/shard_map/reduce_scatter | solution.py:71
  103.3 46.6 %collective-permute-start = (bf16[4,128,128]{1,2,0:T(8,128)(2,1)S(1)}, bf16[4,128,128]{1,2,0:T(8,128)(2,1)S(1)}, u32[]{:S(2)}, u32[]{:S(2)}) collective-permute-start(bf16[4,128,128]{1,2,0:T(8,128)(2,1)S(1)} %get-tuple-element.21), channel_id=1, source_target_pairs={{0,8},{8,16},{16,24},{1,9},{9,17},{17,25},{2,10},{10,18},{18,26},{... | collective-permute-start | bytes 393224 | tf_op jit(solution)/shard_map/ppermute | solution.py:21
  106.7 43.2 %collective-permute-start.1 = (bf16[4,128,128]{1,2,0:T(8,128)(2,1)S(1)}, bf16[4,128,128]{1,2,0:T(8,128)(2,1)S(1)}, u32[]{:S(2)}, u32[]{:S(2)}) collective-permute-start(bf16[4,128,128]{1,2,0:T(8,128)(2,1)S(1)} %get-tuple-element.22), channel_id=1, source_target_pairs={{8,0},{16,8},{24,16},{9,1},{17,9},{25,17},{10,2},{18,10},{26,18},{... | collective-permute-start | bytes 393224 | tf_op jit(solution)/shard_map/ppermute | solution.py:24
  108.0 20.8 %collective-permute-start.3 = (bf16[4,15,128]{1,0,2:T(4,128)(2,1)S(1)}, bf16[4,15,128]{1,0,2:T(4,128)(2,1)S(1)}, u32[]{:S(2)}, u32[]{:S(2)}) collective-permute-start(bf16[4,15,128]{1,0,2:T(4,128)(2,1)S(1)} %get-tuple-element.24), channel_id=1, source_target_pairs={{8,0},{16,8},{24,16},{9,1},{17,9},{25,17},{10,2},{18,10},{26,18},{... | collective-permute-start | bytes 46088 | tf_op jit(solution)/shard_map/ppermute | solution.py:24
  109.4 19.5 %collective-permute-start.2 = (bf16[4,15,128]{1,0,2:T(4,128)(2,1)S(1)}, bf16[4,15,128]{1,0,2:T(4,128)(2,1)S(1)}, u32[]{:S(2)}, u32[]{:S(2)}) collective-permute-start(bf16[4,15,128]{1,0,2:T(4,128)(2,1)S(1)} %get-tuple-element.23), channel_id=1, source_target_pairs={{0,8},{8,16},{16,24},{1,9},{9,17},{17,25},{2,10},{10,18},{18,26},{... | collective-permute-start | bytes 46088 | tf_op jit(solution)/shard_map/ppermute | solution.py:21
Sparse Core Ops, SparseCore 0:
  10.9 48.3 all-gather.7
  61.2 35.3 all-gather.5
  98.2 33.5 all-gather.9
  158.0 48.6 reduce-scatter.1

commit v2 on v1

--- a/solution.py
+++ b/solution.py
@@ -1,8 +1,13 @@
+import functools
+
 import jax
 import jax.numpy as jnp
 from jax import lax
+from jax.experimental import pallas as pl
+from jax.experimental.pallas import tpu as pltpu
 from jax.sharding import PartitionSpec as P
 
+MESH = pl.DeviceIdType.MESH
 HEAD_DIM = 64
 WINDOW = 128
 GRID_W = 64
@@ -51,26 +56,302 @@
     )
 
 
-def gather_inputs(normed, packed_in):
-    return (
-        lax.all_gather(normed, ("fs", "tp"), axis=0, tiled=True),
-        lax.all_gather(packed_in, "sp", axis=0, tiled=True),
-    )
-
-
-def gather_outputs(packed_out, after):
-    return lax.all_gather(packed_out, "sp", axis=1, tiled=True)
+def remote(src, dst, send, recv, **where):
+    return pltpu.make_async_remote_copy(
+        src_ref=src,
+        dst_ref=dst,
+        send_sem=send,
+        recv_sem=recv,
+        device_id=where,
+        device_id_type=MESH,
+    )
+
+
+def meet(peers, waits):
+    barrier = pltpu.get_barrier_semaphore()
+    for condition, where in peers:
+        if condition is None:
+            pl.semaphore_signal(barrier, inc=1, device_id=where, device_id_type=MESH)
+        else:
+
+            @pl.when(condition)
+            def _(where=where):
+                pl.semaphore_signal(barrier, inc=1, device_id=where, device_id_type=MESH)
+
+    pl.semaphore_wait(barrier, waits)
+
+
+def input_kernel(
+    sizes, own_ref, weight_ref, acc_ref, held, whole, local_sem,
+    token_send, token_recv, pass_send, pass_recv, ring_send, ring_recv,
+):
+    n, fs, tp, chunks = sizes
+    me = lax.axis_index("sp")
+    f = lax.axis_index("fs")
+    t = lax.axis_index("tp")
+    depth = weight_ref.shape[0]
+    part = depth // chunks
+    has_left, has_right = me > 0, me < n - 1
+    peers = [(None, {"tp": lax.rem(t + i, tp)}) for i in range(1, tp)]
+    peers += [(None, {"fs": lax.rem(f + j, fs)}) for j in range(1, fs)]
+    peers += [(has_left, {"sp": me - 1}), (has_right, {"sp": me + 1})]
+    meet(peers, tp - 1 + fs - 1 + has_left.astype(jnp.int32) + has_right.astype(jnp.int32))
+
+    def rows(shard, c):
+        return pl.ds(pl.multiple_of(shard * depth + c * part, part), part)
+
+    def ring(side, k, c, shard):
+        source = (
+            weight_ref.at[pl.ds(c * part, part)] if k == 0 else whole.at[rows(shard, c)]
+        )
+        return remote(
+            source, whole.at[rows(shard, c)], ring_send.at[side, k, c],
+            ring_recv.at[side, k, c], sp=(me + 1 if side == 0 else me - 1),
+        )
+
+    def sends(side, k):
+        if side == 0:
+            return jnp.logical_and(me - k >= 0, has_right)
+        return jnp.logical_and(me + k < n, has_left)
+
+    def shard_sent(side, k):
+        return me - k if side == 0 else me + k
+
+    def receives(side, k):
+        return me - 1 - k >= 0 if side == 0 else me + 1 + k < n
+
+    def shard_received(side, k):
+        return me - 1 - k if side == 0 else me + 1 + k
+
+    for c in range(chunks):
+        for side in (0, 1):
+
+            @pl.when(sends(side, 0))
+            def _():
+                ring(side, 0, c, me).start()
+
+    index = f * tp + t
+    token_copies = []
+    for j in range(1, fs):
+        copy = remote(
+            own_ref, held.at[index], token_send.at[j - 1], token_recv.at[j - 1],
+            fs=lax.rem(f + j, fs),
+        )
+        copy.start()
+        token_copies.append(copy)
+    passes = []
+    for i in range(1, tp):
+        copy = remote(
+            own_ref, held.at[index], pass_send.at[0, i - 1], pass_recv.at[0, i - 1],
+            tp=lax.rem(t + i, tp),
+        )
+        copy.start()
+        passes.append(copy)
+    stay_token = pltpu.make_async_copy(own_ref, held.at[index], local_sem.at[0])
+    stay_token.start()
+    stay_weight = pltpu.make_async_copy(
+        weight_ref, whole.at[pl.ds(pl.multiple_of(me * depth, depth), depth)], local_sem.at[1]
+    )
+    stay_weight.start()
+
+    def relay(k):
+        for c in range(chunks):
+            for side in (0, 1):
+
+                @pl.when(receives(side, k))
+                def _():
+                    ring(side, k, c, shard_received(side, k)).wait_recv()
+
+                if k + 1 < n - 1:
+
+                    @pl.when(sends(side, k + 1))
+                    def _():
+                        ring(side, k + 1, c, shard_sent(side, k + 1)).start()
+
+    def tokens_in():
+        for j in range(1, fs):
+            token_copies[j - 1].wait_recv()
+            source = lax.rem(f + fs - j, fs) * tp + t
+            for i in range(1, tp):
+                copy = remote(
+                    held.at[source], held.at[source], pass_send.at[j, i - 1],
+                    pass_recv.at[j, i - 1], tp=lax.rem(t + i, tp),
+                )
+                copy.start()
+                passes.append(copy)
+        stay_token.wait()
+        stay_weight.wait()
+        for copy in passes:
+            copy.wait_recv()
+
+    blocks, height = held.shape[0], held.shape[1]
+
+    def multiply(column, size, first):
+        @pl.loop(0, blocks)
+        def _(b):
+            place = pl.ds(pl.multiple_of(b * height, height), height)
+            term = jnp.dot(
+                held[b, :, pl.ds(column, size)],
+                whole[pl.ds(column, size), :],
+                preferred_element_type=jnp.float32,
+            )
+            if first:
+                acc_ref[place, :] = term
+            else:
+                acc_ref[place, :] += term
+
+    split = depth % 128 == 0
+    early = max(n - 2, 0)
+    for k in range(early):
+        relay(k)
+    tokens_in()
+    if split:
+        multiply(pl.multiple_of(me * depth, depth), depth, True)
+    for k in range(n - 1):
+        if k >= early:
+            relay(k)
+        if split:
+            for side in (0, 1):
+
+                @pl.when(receives(side, k))
+                def _():
+                    shard = shard_received(side, k)
+                    multiply(pl.multiple_of(shard * depth, depth), depth, False)
+
+    if not split:
+        multiply(0, n * depth, True)
+    for copy in token_copies + passes:
+        copy.wait_send()
+    for k in range(n - 1):
+        for c in range(chunks):
+            for side in (0, 1):
+
+                @pl.when(sends(side, k))
+                def _():
+                    ring(side, k, c, shard_sent(side, k)).wait_send()
+
+
+def gather_project(own, weight):
+    n, fs, tp = (lax.axis_size(axis) for axis in ("sp", "fs", "tp"))
+    height, width = own.shape
+    depth, columns = weight.shape
+    chunks = 2 if n <= 8 and depth % 32 == 0 else 1
+    steps = max(n - 1, 1)
+    dma = pltpu.SemaphoreType.DMA
+    return pl.pallas_call(
+        functools.partial(input_kernel, (n, fs, tp, chunks)),
+        out_shape=jax.ShapeDtypeStruct((fs * tp * height, columns), jnp.float32),
+        in_specs=[pl.BlockSpec(memory_space=pltpu.VMEM)] * 2,
+        out_specs=pl.BlockSpec(memory_space=pltpu.VMEM),
+        scratch_shapes=[
+            pltpu.VMEM((fs * tp, height, width), jnp.bfloat16),
+            pltpu.VMEM((n * depth, columns), jnp.bfloat16),
+            dma((2,)),
+            dma((fs - 1,)),
+            dma((fs - 1,)),
+            dma((fs, tp - 1)),
+            dma((fs, tp - 1)),
+            dma((2, steps, chunks)),
+            dma((2, steps, chunks)),
+        ],
+        compiler_params=pltpu.CompilerParams(collective_id=0, has_side_effects=True),
+    )(own, weight)
+
+
+def output_kernel(
+    sizes, feature_ref, weight_ref, out_ref, part_out, part_in, sum_out, sum_in,
+    part_send, part_recv, sum_send, sum_recv,
+):
+    fs, tp = sizes
+    f = lax.axis_index("fs")
+    t = lax.axis_index("tp")
+    height = out_ref.shape[0]
+    peers = [(None, {"tp": lax.rem(t + i, tp)}) for i in range(1, tp)]
+    peers += [(None, {"fs": lax.rem(f + j, fs)}) for j in range(1, fs)]
+    meet(peers, tp - 1 + fs - 1)
+
+    def term(j, i):
+        block = lax.rem(f + j, fs) * tp + lax.rem(t + i, tp)
+        place = pl.ds(pl.multiple_of(block * height, height), height)
+        return jnp.dot(
+            feature_ref[place, :], weight_ref[...], preferred_element_type=jnp.float32
+        )
+
+    order = list(range(fs - 1, -1, -1))
+    copies = {}
+    for j in order:
+        for i in range(1, tp):
+            part_out[i - 1, j] = term(j, i).astype(jnp.bfloat16)
+            copy = remote(
+                part_out.at[i - 1, j], part_in.at[i - 1, j], part_send.at[i - 1, j],
+                part_recv.at[i - 1, j], tp=lax.rem(t + i, tp),
+            )
+            copy.start()
+            copies[i, j] = copy
+    arrivals = []
+    for j in order:
+        total = term(j, 0)
+        for i in range(1, tp):
+            copies[i, j].wait_recv()
+            total = total + part_in[i - 1, j].astype(jnp.float32)
+        if j:
+            sum_out[j - 1] = total.astype(jnp.bfloat16)
+            copy = remote(
+                sum_out.at[j - 1], sum_in.at[j - 1], sum_send.at[j - 1],
+                sum_recv.at[j - 1], fs=lax.rem(f + j, fs),
+            )
+            copy.start()
+            arrivals.append((j, copy))
+    for j, copy in arrivals:
+        copy.wait_recv()
+        total = total + sum_in[j - 1].astype(jnp.float32)
+    out_ref[...] = total.astype(out_ref.dtype)
+    for copy in copies.values():
+        copy.wait_send()
+    for _, copy in arrivals:
+        copy.wait_send()
+
+
+def scatter_sum(features, whole_out):
+    fs, tp = lax.axis_size("fs"), lax.axis_size("tp")
+    width = whole_out.shape[1]
+    height = features.shape[0] // (fs * tp)
+    dma = pltpu.SemaphoreType.DMA
+    return pl.pallas_call(
+        functools.partial(output_kernel, (fs, tp)),
+        out_shape=jax.ShapeDtypeStruct((height, width), jnp.bfloat16),
+        in_specs=[pl.BlockSpec(memory_space=pltpu.VMEM)] * 2,
+        out_specs=pl.BlockSpec(memory_space=pltpu.VMEM),
+        scratch_shapes=[
+            pltpu.VMEM((tp - 1, fs, height, width), jnp.bfloat16),
+            pltpu.VMEM((tp - 1, fs, height, width), jnp.bfloat16),
+            pltpu.VMEM((fs - 1, height, width), jnp.bfloat16),
+            pltpu.VMEM((fs - 1, height, width), jnp.bfloat16),
+            dma((tp - 1, fs)),
+            dma((tp - 1, fs)),
+            dma((fs - 1,)),
+            dma((fs - 1,)),
+        ],
+        compiler_params=pltpu.CompilerParams(collective_id=1, has_side_effects=True),
+    )(features, whole_out)
+
+
+def gather_outputs(packed_out):
+    n = lax.axis_size("sp")
+    if n > 8:
+        return lax.all_gather(packed_out, "sp", axis=1, tiled=True)
+    me = lax.axis_index("sp")
+    pieces = [packed_out]
+    for k in range(1, n):
+        pieces.append(lax.ppermute(packed_out, "sp", [(i, (i + k) % n) for i in range(n)]))
+    pieces = pieces[::-1]
+    lined = jnp.concatenate(pieces + pieces[:-1], axis=1)
+    width = packed_out.shape[1]
+    return lax.dynamic_slice_in_dim(lined, lax.rem(n - 1 - me, n) * width, n * width, 1)
 
 
 def gather_stats(pair):
     return lax.all_gather(pair, ("fs", "tp"), axis=0)
-
-
-def scatter_sum(features, whole_out):
-    partial = jnp.dot(features, whole_out, preferred_element_type=jnp.float32)
-    return lax.psum_scatter(
-        partial.astype(jnp.bfloat16), ("fs", "tp"), scatter_dimension=0, tiled=True
-    )
 
 
 def local(
@@ -138,9 +419,9 @@
         ],
         axis=0,
     )
-    whole_normed, whole_in = gather_inputs(normed, packed_in)
-    whole_out = gather_outputs(packed_out, whole_in)
-    acc = jnp.dot(whole_normed, whole_in, preferred_element_type=jnp.float32)
+    acc = gather_project(normed, packed_in)
+    acc, packed_out = lax.optimization_barrier((acc, packed_out))
+    whole_out = gather_outputs(packed_out)
     cut = [head_cols, head_cols + chan_cols, head_cols + 2 * chan_cols]
     cut.append(cut[2] + kv_cols)
     tokens_here = fs_count * rows_here

time: 214 us -> 152 us (0.71)
  waiting for transfers between devices: 138 us -> 0.02 us
  Pallas kernels: 0 us -> 76.6 us
  local copies, waits for them, and re-layouts: 10.7 us -> 23.9 us
  between operations: 13.6 us -> 0.48 us
  matrix products: 11.8 us -> 2.06 us
  starting transfers between devices: 11.3 us -> 16.9 us
  other arithmetic: 18.2 us -> 22.4 us
    pallas_call x0 -> x2, Pallas kernels: none -> 76.6 us  [the longest x1 44.4 us: gather_project(): pl.pallas_call(functools.partial(input_kernel, (n, fs, tp, chunks)), out_...]
    all_gather x3 -> x0, waiting for transfers between devices: 75.2 us -> none  [the longest x1 37.9 us: gather_inputs(): lax.all_gather(packed_in, 'sp', axis=0, tiled=True)]
    reduce_scatter x1 -> x0, waiting for transfers between devices: 48.8 us -> none  [scatter_sum(): lax.psum_scatter(partial.astype(jnp.bfloat16), ('fs', 'tp'), scatter_dime...]
    ppermute x2, waiting for transfers between devices: 14.2 us -> 0.01 us  [padded(): lax.ppermute(lax.slice_in_dim(block, 0, width, axis=dim), axis, backward)]
    dot_general x2 -> x0, matrix products: 9.72 us -> none  [the longest x1 5.24 us: local(): acc = jnp.dot(whole_normed, whole_in, preferred_element_type=jnp.float32)]
    reduce_sum x1, other arithmetic: 10.7 us -> 3.88 us  [local(): own_mean = jnp.mean(filtered, axis=-1)]
    another operation x2, other arithmetic: 0.63 us -> 6.54 us
    concatenate x8, local copies, waits for them, and re-layouts: 0.1 us -> 5.78 us  [grid_rotate(): jnp.concatenate([rotate_pairs(values[..., :middle], positions // GRID_W),...]
  transfers between devices with their start and end apart: 8 -> 7, of which waited for: 4 -> 0; matrix products, arithmetic and copies ran while one was open for 15% -> 25% of each run, Pallas kernels for 0% -> 0%
where the time goes in v2:
time: 152 us; the launch traced here: 151 us
  Pallas kernels  76.6 us (50%)
  local copies, waits for them, and re-layouts  23.9 us (16%)
  other arithmetic  22.4 us (15%)
  starting transfers between devices  16.9 us (11%)
  blocking collectives  8.57 us (6%)
  matrix products  2.06 us (1%)
    pallas_call x1, Pallas kernels, gather_project(): pl.pallas_call(functools.partial(input_kernel, (n, fs, tp, chunks)), out_...  44.4 us
    pallas_call x1, Pallas kernels, scatter_sum(): pl.pallas_call(functools.partial(output_kernel, (fs, tp)), out_shape=jax....  32.1 us
    ppermute x2, starting transfers between devices, padded(): lax.ppermute(lax.slice_in_dim(block, block.shape[dim] - width, None, axis...  11.2 us
    all_gather x1, blocking collectives, gather_stats(): return lax.all_gather(pair, ('fs', 'tp'), axis=0)  8.57 us
    another operation x2, other arithmetic  6.54 us
    concatenate x8, local copies, waits for them, and re-layouts, grid_rotate(): jnp.concatenate([rotate_pairs(values[..., :middle], positions // GRID_W),...  5.78 us
    dynamic_slice x8, local copies, waits for them, and re-layouts, columns(): return lax.dynamic_slice_in_dim(array, start, size, axis % array.ndim)  5.68 us
    reduce_sum x1, other arithmetic, local(): own_mean = jnp.mean(filtered, axis=-1)  3.88 us
  transfers between devices with their start and end apart: 7, of which 0 were waited for; matrix products, arithmetic and copies ran while one was open for 25% of the time, Pallas kernels for 0%

profile of v2, /device:TPU:0, one launch (start us, length us, event | category | flops | bytes accessed | tf_op | source)
XLA Modules:
  0.0 150.9 jit_solution(9533442640530799247)
XLA Ops:
  0.0 1.3 fusion.10
  1.3 2.0 %fusion.12.own_ref = bf16[128,2048]{1,0:T(8,128)(2,1)} fusion(f32[2048]{0:T(1024)} %param.15, f32[128]{0:T(128)S(1)} %add_rsqrt_fusion.1, bf16[256,2048]{1,0:T(8,128)(2,1)} %param.14, s32[]{:T(128)S(6)} %select_n.68), kind=kLoop, calls=%fused_computation.41 | loop fusion | flops 1048576 | bytes 1057284 | tf_op jit(solution)/shard_map/convert_element_type | solution.py:404
  3.4 1.0 constant_dynamic-slice_fusion.6
  4.6 1.0 concatenate.81.weight_ref
  5.6 44.4 %shard_map.136 = f32[1024,512]{1,0:T(8,128)} custom-call(bf16[128,2048]{1,0:T(8,128)(2,1)} %fusion.12.own_ref, bf16[512,512]{1,0:T(8,128)(2,1)} %concatenate.81.weight_ref), custom_call_target="tpu_custom_call" | custom-call | tf_op jit(solution)/shard_map/pallas_call | solution.py:241
  50.0 1.0 constant_dynamic-slice_fusion.2
  51.0 2.5 %collective-permute-start.4 = (bf16[256,512]{1,0:T(8,128)(2,1)S(1)}, bf16[256,512]{1,0:T(8,128)(2,1)S(1)}, u32[]{:S(2)}, u32[]{:S(2)}) collective-permute-start(bf16[256,512]{1,0:T(8,128)(2,1)S(1)} %pad_maximum_fusion.4), channel_id=1, source_target_pairs={{0,24},{8,0},{16,8},{24,16},{1,25},{9,1},{17,9},{25,17},{2,26},{10... | collective-permute-start | bytes 786440 | tf_op jit(solution)/shard_map/ppermute | solution.py:346
  53.6 0.6 collective-permute-start.6
  54.2 1.5 %fusion.88 = (f32[1024,128]{1,0:T(8,128)S(1)}, bf16[1024,128]{1,0:T(8,128)(2,1)S(1)}) fusion(f32[1024,512]{1,0:T(8,128)} %shard_map.136), kind=kLoop, calls=%fused_computation.236 | loop fusion | flops 655360 | bytes 2359296 | tf_op jit(solution)/shard_map/slice | solution.py:429
  55.7 0.6 fusion.90
  56.3 1.3 collective-permute-start.3
  57.6 6.0 %collective-permute-start.2 = (bf16[4,15,128]{2,1,0:T(8,128)(2,1)}, bf16[4,15,128]{2,1,0:T(8,128)(2,1)}, u32[]{:S(2)}, u32[]{:S(2)}) collective-permute-start(bf16[4,15,128]{2,1,0:T(8,128)(2,1)} %get-tuple-element.27), channel_id=1, source_target_pairs={{0,8},{8,16},{16,24},{1,9},{9,17},{17,25},{2,10},{10,18},{18,26},{... | collective-permute-start | bytes 46088 | tf_op jit(solution)/shard_map/ppermute | solution.py:26
  63.6 0.6 iota_add_fusion.1
  64.2 0.6 iota_add_fusion
  64.8 0.6 fusion.80
  65.4 1.1 slice_bitcast_fusion
  66.5 1.9 %slice.672 = bf16[1024,64]{1,0:T(8,128)(2,1)} slice(f32[1024,512]{1,0:T(8,128)} %shard_map.136), slice={[0:1024], [448:512]} | slice | bytes 262144 | tf_op jit(solution)/shard_map/slice | solution.py:433
  68.6 1.2 multiply_cosine_fusion.3
  69.8 5.5 %fusion.24 = (bf16[1024,1,16]{2,0,1:T(8,128)(2,1)S(1)}, bf16[1024,1,16]{2,0,1:T(8,128)(2,1)}, bf16[1024,1,16]{2,0,1:T(8,128)(2,1)}, bf16[1024,1,16]{2,0,1:T(8,128)(2,1)}) fusion(f32[1024,1,64]{2,0,1:T(8,128)S(1)} %slice_bitcast_fusion, f32[1024]{0:T(1024)S(1)} %get-tuple-element.74, f32[16]{0:T(128)S(1)} %multiply_power_fusion, f32[1024]{0:T(1024)S(1)} %get-tuple-element.73), kind=kLoop, calls=%fused_computation.57 | loop fusion | flops 294912 | bytes 401472 | tf_op jit(solution)/shard_map/convert.13
  75.4 1.1 copy.53
  76.4 1.1 copy.54
  77.5 1.1 copy.55
  78.9 0.7 fusion.89
  79.9 1.0 subtract_convert_fusion.1
  80.9 1.1 fusion.82
  82.1 1.1 dynamic-slice_bitcast_fusion.29
  83.1 0.8 dynamic_slice.51
  83.9 0.8 dynamic_slice.54
  84.6 0.8 dynamic_slice.53
  85.4 0.6 copy.90
  86.0 0.6 copy.91
  86.6 0.6 copy.92
  87.3 0.6 copy.93
  87.9 1.3 dynamic_slice.50
  89.2 1.3 collective-permute-start.1
  90.5 5.2 %collective-permute-start = (bf16[4,128,128]{1,2,0:T(8,128)(2,1)}, bf16[4,128,128]{1,2,0:T(8,128)(2,1)}, u32[]{:S(2)}, u32[]{:S(2)}) collective-permute-start(bf16[4,128,128]{1,2,0:T(8,128)(2,1)} %get-tuple-element.25), channel_id=1, source_target_pairs={{0,8},{8,16},{16,24},{1,9},{9,17},{17,25},{2,10},{10,18},{18,26},{... | collective-permute-start | bytes 393224 | tf_op jit(solution)/shard_map/ppermute | solution.py:26
  95.7 3.9 %fusion.87 = (f32[4,256]{1,0:T(4,128)S(1)}, f32[4,256,128]{2,1,0:T(8,128)S(1)}) fusion(bf16[4,15,128]{2,1,0:T(8,128)(2,1)S(1)} %collective-permute-done.3, bf16[4,256,128]{2,1,0:T(8,128)(2,1)S(1)} %bitcast.155, f32[128]{0:T(128)S(1)} %get-tuple-element.62, f32[128]{0:T(128)S(1)} %get-tuple-element.33, f32[128]{0:T(128)S(1)} %get-tuple-element.34, ...), kind=kLoop, calls=%fused_computation.235 | loop fusion | flops 24116224 | bytes 837632 | tf_op jit(solution)/shard_map/reduce_sum | solution.py:448
  100.0 8.6 %all-gather.1 = f32[8,2,1024]{2,1,0:T(2,128)S(1)} all-gather(f32[1,2,1024]{2,1,0:T(2,128)S(1)} %maximum_bitcast_fusion), channel_id=2, replica_groups=mesh['sp'=4,'fs'=4,'tp'=2] {'fs','tp'}, dimensions={0}, use_global_device_ids=true | all-gather | bytes 73728 | tf_op jit(solution)/shard_map/all_gather | solution.py:354
  109.1 0.6 copy-done.4
  109.8 1.0 pad_maximum_fusion
  110.9 0.8 fusion.1
  111.8 0.9 fusion
  112.7 1.2 fusion.7
  114.0 0.4 copy.70
  114.6 0.9 pad_maximum_fusion.1.feature_ref
  115.7 1.1 constant_dynamic-slice_fusion.1.weight_ref
  116.8 32.1 %shard_map.137 = bf16[128,2048]{1,0:T(8,128)(2,1)} custom-call(bf16[1024,256]{1,0:T(8,128)(2,1)} %pad_maximum_fusion.1.feature_ref, bf16[256,2048]{1,0:T(8,128)(2,1)} %constant_dynamic-slice_fusion.1.weight_ref), custom_call_target="tpu_custom_call" | custom-call | tf_op jit(solution)/shard_map/pallas_call | solution.py:320
  149.0 1.9 %copy.105 = bf16[128,2048]{1,0:T(8,128)(2,1)} copy(bf16[128,2048]{1,0:T(8,128)(2,1)} %shard_map.137) | data formatting | bytes 1048576
  (72 shorter events, 2.5 us)
Async XLA Ops:
  0.0 3.4 %copy-start = (bf16[512,512]{1,0:T(8,128)(2,1)S(1)}, bf16[512,512]{1,0:T(8,128)(2,1)}, u32[]{:S(2)}) copy-start(bf16[512,512]{1,0:T(8,128)(2,1)} %param.16) | copy-start | bytes 1572868
  0.0 4.4 %copy-start.2 = (bf16[512,128]{1,0:T(8,128)(2,1)S(1)}, bf16[512,128]{1,0:T(8,128)(2,1)}, u32[]{:S(2)}) copy-start(bf16[512,128]{1,0:T(8,128)(2,1)} %param.18) | copy-start | bytes 393220
  0.0 4.4 %copy-start.3 = (bf16[512,128]{1,0:T(8,128)(2,1)S(1)}, bf16[512,128]{1,0:T(8,128)(2,1)}, u32[]{:S(2)}) copy-start(bf16[512,128]{1,0:T(8,128)(2,1)} %param.17) | copy-start | bytes 393220
  51.0 64.5 %collective-permute-start.4 = (bf16[256,512]{1,0:T(8,128)(2,1)S(1)}, bf16[256,512]{1,0:T(8,128)(2,1)S(1)}, u32[]{:S(2)}, u32[]{:S(2)}) collective-permute-start(bf16[256,512]{1,0:T(8,128)(2,1)S(1)} %pad_maximum_fusion.4), channel_id=1, source_target_pairs={{0,24},{8,0},{16,8},{24,16},{1,25},{9,1},{17,9},{25,17},{2,26},{10... | collective-permute-start | bytes 786440 | tf_op jit(solution)/shard_map/ppermute | solution.py:346
  53.6 62.0 %collective-permute-start.5 = (bf16[256,512]{1,0:T(8,128)(2,1)S(1)}, bf16[256,512]{1,0:T(8,128)(2,1)S(1)}, u32[]{:S(2)}, u32[]{:S(2)}) collective-permute-start(bf16[256,512]{1,0:T(8,128)(2,1)S(1)} %pad_maximum_fusion.4), channel_id=1, source_target_pairs={{0,16},{8,24},{16,0},{24,8},{1,17},{9,25},{17,1},{25,9},{2,18},{10... | collective-permute-start | bytes 786440 | tf_op jit(solution)/shard_map/ppermute | solution.py:346
  53.6 62.0 %collective-permute-start.6 = (bf16[256,512]{1,0:T(8,128)(2,1)S(1)}, bf16[256,512]{1,0:T(8,128)(2,1)S(1)}, u32[]{:S(2)}, u32[]{:S(2)}) collective-permute-start(bf16[256,512]{1,0:T(8,128)(2,1)S(1)} %pad_maximum_fusion.4), channel_id=1, source_target_pairs={{0,8},{8,16},{16,24},{24,0},{1,9},{9,17},{17,25},{25,1},{2,10},{10... | collective-permute-start | bytes 786440 | tf_op jit(solution)/shard_map/ppermute | solution.py:346
  56.3 32.8 %collective-permute-start.3 = (bf16[4,15,128]{2,1,0:T(8,128)(2,1)}, bf16[4,15,128]{2,1,0:T(8,128)(2,1)S(1)}, u32[]{:S(2)}, u32[]{:S(2)}) collective-permute-start(bf16[4,15,128]{2,1,0:T(8,128)(2,1)} %get-tuple-element.28), channel_id=1, source_target_pairs={{8,0},{16,8},{24,16},{9,1},{17,9},{25,17},{10,2},{18,10},{26,18},{... | collective-permute-start | bytes 46088 | tf_op jit(solution)/shard_map/ppermute | solution.py:29
  57.6 32.8 %collective-permute-start.2 = (bf16[4,15,128]{2,1,0:T(8,128)(2,1)}, bf16[4,15,128]{2,1,0:T(8,128)(2,1)}, u32[]{:S(2)}, u32[]{:S(2)}) collective-permute-start(bf16[4,15,128]{2,1,0:T(8,128)(2,1)} %get-tuple-element.27), channel_id=1, source_target_pairs={{0,8},{8,16},{16,24},{1,9},{9,17},{17,25},{2,10},{10,18},{18,26},{... | collective-permute-start | bytes 46088 | tf_op jit(solution)/shard_map/ppermute | solution.py:26
  69.8 8.9 %copy-start.1 = (bf16[1024,64]{1,0:T(8,128)(2,1)S(1)}, bf16[1024,64]{1,0:T(8,128)(2,1)}, u32[]{:S(2)}) copy-start(bf16[1024,64]{1,0:T(8,128)(2,1)} %slice.672) | copy-start | bytes 393220
  75.3 4.3 %copy-start.9 = (s32[512]{0:T(512)S(1)}, s32[512]{0:T(512)}, u32[]{:S(2)}) copy-start(s32[512]{0:T(512)} %iota_add_fusion) | copy-start | bytes 6148
  75.3 4.3 %copy-start.11 = (s32[256]{0:T(256)S(1)}, s32[256]{0:T(256)}, u32[]{:S(2)}) copy-start(s32[256]{0:T(256)} %iota_add_fusion.1) | copy-start | bytes 3076
  75.3 4.3 %copy-start.12 = (pred[512]{0:T(512)(128)(4,1)S(1)}, pred[512]{0:T(512)(128)(4,1)}, u32[]{:S(2)}) copy-start(pred[512]{0:T(512)(128)(4,1)} %get-tuple-element.81) | copy-start | bytes 1540
  75.3 4.3 %copy-start.13 = (pred[512]{0:T(512)(128)(4,1)S(1)}, pred[512]{0:T(512)(128)(4,1)}, u32[]{:S(2)}) copy-start(pred[512]{0:T(512)(128)(4,1)} %get-tuple-element.82) | copy-start | bytes 1540
  89.2 19.9 %collective-permute-start.1 = (bf16[4,128,128]{1,2,0:T(8,128)(2,1)}, bf16[4,128,128]{1,2,0:T(8,128)(2,1)S(1)}, u32[]{:S(2)}, u32[]{:S(2)}) collective-permute-start(bf16[4,128,128]{1,2,0:T(8,128)(2,1)} %get-tuple-element.26), channel_id=1, source_target_pairs={{8,0},{16,8},{24,16},{9,1},{17,9},{25,17},{10,2},{18,10},{26,18},{... | collective-permute-start | bytes 393224 | tf_op jit(solution)/shard_map/ppermute | solution.py:29
  90.5 19.3 %collective-permute-start = (bf16[4,128,128]{1,2,0:T(8,128)(2,1)}, bf16[4,128,128]{1,2,0:T(8,128)(2,1)}, u32[]{:S(2)}, u32[]{:S(2)}) collective-permute-start(bf16[4,128,128]{1,2,0:T(8,128)(2,1)} %get-tuple-element.25), channel_id=1, source_target_pairs={{0,8},{8,16},{16,24},{1,9},{9,17},{17,25},{2,10},{10,18},{18,26},{... | collective-permute-start | bytes 393224 | tf_op jit(solution)/shard_map/ppermute | solution.py:26
  99.5 11.3 %copy-start.5 = (bf16[2,2,4,8,256]{4,3,1,0,2:T(8,128)(2,1)S(1)}, bf16[2,2,4,8,256]{4,3,1,0,2:T(8,128)(2,1)}, u32[]{:S(2)}) copy-start(bf16[2,2,4,8,256]{4,3,1,0,2:T(8,128)(2,1)} %copy.90) | copy-start | bytes 196612
  99.6 11.3 %copy-start.6 = (bf16[2,2,4,8,256]{4,3,1,0,2:T(8,128)(2,1)S(1)}, bf16[2,2,4,8,256]{4,3,1,0,2:T(8,128)(2,1)}, u32[]{:S(2)}) copy-start(bf16[2,2,4,8,256]{4,3,1,0,2:T(8,128)(2,1)} %copy.91) | copy-start | bytes 196612
  99.6 11.3 %copy-start.7 = (bf16[2,2,4,8,256]{4,3,1,0,2:T(8,128)(2,1)S(1)}, bf16[2,2,4,8,256]{4,3,1,0,2:T(8,128)(2,1)}, u32[]{:S(2)}) copy-start(bf16[2,2,4,8,256]{4,3,1,0,2:T(8,128)(2,1)} %copy.92) | copy-start | bytes 196612
  99.6 11.3 %copy-start.8 = (bf16[2,2,4,8,256]{4,3,1,0,2:T(8,128)(2,1)S(1)}, bf16[2,2,4,8,256]{4,3,1,0,2:T(8,128)(2,1)}, u32[]{:S(2)}) copy-start(bf16[2,2,4,8,256]{4,3,1,0,2:T(8,128)(2,1)} %copy.93) | copy-start | bytes 196612
  109.1 0.7 copy-start.4
  110.8 0.8 copy-start.10
